TPU v7x, 32 devices: a whole 2x2x4 slice. The times are simulated.
32 devices in a mesh: row: 8 (over z, x), col: 4 (over y, core).
Axes of the slice: x: 2, y: 2, z: 4, core: 2. Of those that a mesh axis runs over, the one named last changes fastest.
Arguments:
- tokens: bfloat16 [9216, 4096], P('row'), may hold values from -6 to 6
- proj_in: bfloat16 [4096, 512], P(None, 'col'), may hold values from -0.09375 to 0.09375
- proj_out: bfloat16 [512, 4096], P(None, 'col'), may hold values from -0.25 to 0.25
Outputs:
- mixed: bfloat16 [9216, 4096], P('row', 'col')
All inputs are finite; a program needn't handle non-finite values.
Results may differ from a plain program's by a relative error of at most 0.0057.
Values may be sent and summed in bfloat16 or wider, within the bound.
No kernel may reach another device: no remote copies, remote signals or barrier semaphores. Data moves between devices by JAX's collectives and lax.ppermute only.
A program may use at most 64 MiB of HBM per device.

v0:
```python
import math

import jax
import jax.numpy as jnp
import numpy as np
from jax import lax
from jax.experimental import pallas as pl
from jax.experimental.pallas import tpu as pltpu
from jax.sharding import Mesh, PartitionSpec as P

LANES = 128
ROW = "row"
COL = ("far", "near")
CHUNKS = 1


def cos_sin(row_ids, col_ids, period):
    phase_idx = row_ids * col_ids % period
    angles = phase_idx.astype(jnp.float32) * (2.0 * math.pi / period)
    return (jnp.cos(angles), jnp.sin(angles))


def apply_table(form, table_cos, table_sin, real_part, imag_part):
    highest = lax.Precision.HIGHEST
    out_real = jnp.einsum(form, table_cos, real_part, precision=highest) + jnp.einsum(
        form, table_sin, imag_part, precision=highest
    )
    out_imag = jnp.einsum(form, table_cos, imag_part, precision=highest) - jnp.einsum(
        form, table_sin, real_part, precision=highest
    )
    return (out_real, out_imag)


def general_device(tokens, proj_in, proj_out):
    row_count = lax.axis_size(ROW)
    local_rows = tokens.shape[0]
    group_width = proj_in.shape[1]
    seq_length = local_rows * row_count
    row_rank = lax.axis_index(ROW)
    highest = lax.Precision.HIGHEST
    first_len = 16
    second_len = local_rows // first_len
    branch_in = jnp.dot(tokens, proj_in, preferred_element_type=jnp.float32).astype(jnp.bfloat16)
    outer_idx = jnp.arange(row_count, dtype=jnp.int32)
    outer_cos, outer_sin = cos_sin(outer_idx[:, None], outer_idx[None, :], row_count)
    values = lax.all_to_all(
        branch_in.reshape(1, local_rows, group_width),
        "row",
        split_axis=1,
        concat_axis=0,
        tiled=True,
    ).astype(jnp.float32)
    real_part = jnp.einsum("kn,nmg->kmg", outer_cos, values, precision=highest)
    imag_part = -jnp.einsum("kn,nmg->kmg", outer_sin, values, precision=highest)
    real_parts = real_part
    imag_parts = imag_part
    inner_idx = jnp.arange(local_rows, dtype=jnp.int32)
    first_idx = jnp.arange(first_len, dtype=jnp.int32)
    second_idx = jnp.arange(second_len, dtype=jnp.int32)
    first_cos, first_sin = cos_sin(first_idx[:, None], first_idx[None, :], first_len)
    second_cos, second_sin = cos_sin(second_idx[:, None], second_idx[None, :], second_len)
    mid_cos, mid_sin = cos_sin(first_idx[:, None], second_idx[None, :], local_rows)
    mid_cos = mid_cos[None, :, :, None]
    mid_sin = mid_sin[None, :, :, None]
    twid_cos, twid_sin = cos_sin(row_rank, inner_idx, seq_length)
    twid_cos = twid_cos[None, :, None]
    twid_sin = twid_sin[None, :, None]
    real_part = lax.all_to_all(real_parts, "row", split_axis=0, concat_axis=1, tiled=True)
    imag_part = lax.all_to_all(imag_parts, "row", split_axis=0, concat_axis=1, tiled=True)
    real_part, imag_part = (
        real_part * twid_cos + imag_part * twid_sin,
        imag_part * twid_cos - real_part * twid_sin,
    )
    leading = real_part.shape[0]
    items = real_part.shape[2]
    real_part = real_part.reshape(leading, first_len, second_len, items)
    imag_part = imag_part.reshape(leading, first_len, second_len, items)
    real_part, imag_part = apply_table("kn,anqg->akqg", first_cos, first_sin, real_part, imag_part)
    real_part, imag_part = (
        real_part * mid_cos + imag_part * mid_sin,
        imag_part * mid_cos - real_part * mid_sin,
    )
    real_part, imag_part = apply_table(
        "kq,apqg->akpg", second_cos, second_sin, real_part, imag_part
    )
    spec_real = real_part.reshape(leading, local_rows, items)
    spec_imag = imag_part.reshape(leading, local_rows, items)
    channel = jnp.arange(group_width, dtype=jnp.int32)
    chan_cos, chan_sin = cos_sin(channel[:, None], channel[None, :], group_width)
    norm_scale = 1.0 / math.sqrt(seq_length * group_width)
    mixed_real = (
        jnp.dot(
            spec_real.reshape(local_rows, group_width),
            chan_cos,
            precision=highest,
            preferred_element_type=jnp.float32,
        )
        + jnp.dot(
            spec_imag.reshape(local_rows, group_width),
            chan_sin,
            precision=highest,
            preferred_element_type=jnp.float32,
        )
    ) * norm_scale
    spectrum = mixed_real.astype(jnp.bfloat16)
    returned = lax.all_to_all(
        spectrum.reshape(local_rows, 1, group_width), "row", split_axis=0, concat_axis=1, tiled=True
    )
    returned = returned.reshape(local_rows, group_width)
    output_sum = jnp.dot(
        lax.all_gather(returned, COL, axis=1, tiled=True),
        proj_out,
        preferred_element_type=jnp.float32,
    )
    return output_sum.astype(jnp.bfloat16)


def scaled(value, factor):
    if value is None or abs(factor) < 1e-9:
        return None
    if abs(factor - 1) < 1e-9:
        return value
    if abs(factor + 1) < 1e-9:
        return -value
    return value * np.float32(factor)


def plus(left, right):
    if left is None:
        return right
    return left if right is None else left + right


def minus(left, right):
    if right is None:
        return left
    return -right if left is None else left - right


def complex_scaled(value, angle):
    real, imag = value
    cos, sin = math.cos(angle), math.sin(angle)
    return (
        plus(scaled(real, cos), scaled(imag, sin)),
        minus(scaled(imag, cos), scaled(real, sin)),
    )


def half_transform(values):
    count = len(values)
    half = (count - 1) // 2
    evens = [plus(values[n], values[count - n]) for n in range(1, half + 1)]
    odds = [minus(values[n], values[count - n]) for n in range(1, half + 1)]
    sums = []
    for k in range(count // 2 + 1):
        cos_sum, sin_sum = values[0], None
        if count % 2 == 0:
            cos_sum = plus(cos_sum, scaled(values[count // 2], (-1.0) ** k))
        for n in range(1, half + 1):
            angle = 2 * math.pi * (n * k % count) / count
            cos_sum = plus(cos_sum, scaled(evens[n - 1], math.cos(angle)))
            sin_sum = plus(sin_sum, scaled(odds[n - 1], math.sin(angle)))
        sums.append((cos_sum, sin_sum))
    return sums


def transform(values):
    count = len(values)
    real = half_transform([v[0] for v in values])
    imag = half_transform([v[1] for v in values])
    result = [None] * count
    for k in range(count // 2 + 1):
        (real_cos, real_sin), (imag_cos, imag_sin) = real[k], imag[k]
        result[k] = (plus(real_cos, imag_sin), minus(imag_cos, real_sin))
        if 0 < k < count - k:
            result[count - k] = (minus(real_cos, imag_sin), plus(imag_cos, real_sin))
    return result


def narrow(table):
    return table.astype(jnp.bfloat16)


def split(table):
    high = narrow(table)
    return high, narrow(table - high.astype(np.float64))


def channel_table(width):
    channel = np.arange(width)
    cosines = np.arange(width // 2 + 1)
    sines = np.arange(1, width // 2)
    angle = 2 * math.pi / width
    rows = [
        np.cos(angle * (cosines[:, None] * channel % width)),
        np.sin(angle * (sines[:, None] * channel % width)),
    ]
    return np.concatenate(rows) / math.sqrt(width)


def unpack_table(width, ranks, chunks):
    table = np.zeros((width, width))
    for k in range(width // 2 + 1):
        table[k, k] = table[k, -k % width] = 1
    for k in range(1, width // 2):
        row = width // 2 + k
        table[row, k], table[row, width - k] = -1, 1
    table = table.reshape(ranks, chunks, -1, width).transpose(1, 0, 2, 3)
    return table.reshape(width, width)


def in_vmem(array):
    return pltpu.with_memory_space_constraint(array, pltpu.VMEM)


def in_hbm(array):
    return pltpu.with_memory_space_constraint(array, pltpu.HBM)


VMEM_SPEC = pl.BlockSpec(memory_space=pltpu.VMEM)
SMEM_SPEC = pl.BlockSpec(memory_space=pltpu.SMEM)
PARAMS = pltpu.CompilerParams(vmem_limit_bytes=32 * 2**20)


def project_in(tokens, proj_in):
    rows, width = tokens.shape
    group = proj_in.shape[1]
    high, low = split(channel_table(group))
    steps = 2 if width % 256 == 0 else 1
    depth = width // steps

    def body(tokens_ref, proj_ref, high_ref, low_ref, out_ref, sum_ref):
        step = pl.program_id(0)
        part = jnp.dot(
            tokens_ref[...], proj_ref[...], preferred_element_type=jnp.float32
        )

        @pl.when(step == 0)
        def _():
            sum_ref[...] = part

        @pl.when(step > 0)
        def _():
            sum_ref[...] += part

        @pl.when(step == steps - 1)
        def _():
            branch = sum_ref[...].astype(jnp.bfloat16)
            dims = (((1,), (1,)), ((), ()))
            packed = lax.dot_general(
                high_ref[...], branch, dims, preferred_element_type=jnp.float32
            ) + lax.dot_general(low_ref[...], branch, dims, preferred_element_type=jnp.float32)
            out_ref[...] = packed.astype(jnp.bfloat16)

    whole = lambda i: (0, 0)
    return pl.pallas_call(
        body,
        grid=(steps,),
        in_specs=[
            pl.BlockSpec((rows, depth), lambda i: (0, i)),
            pl.BlockSpec((depth, group), lambda i: (i, 0)),
            pl.BlockSpec((group, group), whole),
            pl.BlockSpec((group, group), whole),
        ],
        out_specs=pl.BlockSpec((group, rows), whole),
        out_shape=jax.ShapeDtypeStruct((group, rows), jnp.bfloat16),
        scratch_shapes=[pltpu.VMEM((rows, group), jnp.float32)],
        compiler_params=PARAMS,
        name="project_in",
    )(*map(in_hbm, (tokens, proj_in, jnp.asarray(high), jnp.asarray(low))))


def sequence_transform(values, first_packed, group, chunk, chunks):
    ranks, items, local = values.shape
    items //= chunks
    offset = chunk * items
    tiles = local // LANES
    coarse = ranks * tiles
    length = ranks * local
    blocks = LANES // ranks
    parts = 8
    groups = coarse // parts
    lane = np.arange(LANES)
    twiddle = 2 * math.pi / length * np.arange(coarse)[:, None] * lane
    fine = np.zeros((parts, 2 * LANES, LANES))
    for part in range(parts):
        for rank in range(ranks):
            for block in range(blocks):
                angle = 2 * math.pi / LANES * (lane * (blocks * rank + block) % LANES)
                at = parts * block + (part + rank) % parts
                fine[part, :, at] = np.concatenate([np.cos(angle), np.sin(angle)])
    fine = narrow(fine / math.sqrt(length))

    def body(first_ref, values_ref, cos_ref, sin_ref, fine_ref, out_ref, work_ref):
        packed = first_ref[0] + offset + lax.broadcasted_iota(jnp.int32, (items, LANES), 0)
        turned = packed > group // 2
        outer = []
        for tile in range(tiles):
            at = pl.ds(tile * LANES, LANES)
            outer.append(
                half_transform(
                    [values_ref[rank, offset : offset + items, at].astype(jnp.float32) for rank in range(ranks)]
                )
            )

        def put(c, real, imag):
            cos, sin = cos_ref[c : c + 1, :], sin_ref[c : c + 1, :]
            real, imag = real * cos + imag * sin, imag * cos - real * sin
            real, imag = jnp.where(turned, -imag, real), jnp.where(turned, real, imag)
            part, at = c % parts, pl.ds(c // parts * items, items)
            work_ref[part, at, :LANES] = real.astype(jnp.bfloat16)
            work_ref[part, at, LANES:] = imag.astype(jnp.bfloat16)

        zero = jnp.zeros((items, LANES), jnp.float32)
        for k in range(ranks // 2 + 1):
            column = []
            for tile in range(tiles):
                cos_sum, sin_sum = outer[tile][k]
                column.append(complex_scaled((cos_sum, scaled(sin_sum, -1.0)), 2 * math.pi * k * tile / coarse))
            for m, (real, imag) in enumerate(transform(column)):
                c = k + ranks * m
                mirror = (coarse - c) % coarse
                real = zero if real is None else real
                imag = zero if imag is None else imag
                if mirror % ranks == k and mirror < c:
                    continue
                put(c, real, imag)
                if mirror != c:
                    put(mirror, real, -imag)

        found = [
            jnp.dot(work_ref[part], fine_ref[part], preferred_element_type=jnp.float32)
            for part in range(parts)
        ]
        low_lane = lax.broadcasted_iota(jnp.int32, (groups * items, LANES), 1) % parts
        for rank in range(ranks):
            level = [found[(e - rank) % parts] for e in range(parts)]
            bit = 1
            while len(level) > 1:
                odd = (low_lane & bit) != 0
                level = [jnp.where(odd, b, a) for a, b in zip(level[::2], level[1::2])]
                bit *= 2
            merged = level[0]
            turn = rank % parts
            if turn:
                merged = jnp.where(
                    low_lane < parts - turn,
                    pltpu.roll(merged, LANES - turn, 1),
                    pltpu.roll(merged, parts - turn, 1),
                )
            merged = merged.astype(jnp.bfloat16)
            for tile in range(groups):
                out_ref[rank, :, pl.ds(tile * LANES, LANES)] = merged[tile * items : (tile + 1) * items]

    return pl.pallas_call(
        body,
        in_specs=[SMEM_SPEC] + [VMEM_SPEC] * 4,
        out_specs=VMEM_SPEC,
        out_shape=pltpu.VMEM((ranks, items, local), jnp.bfloat16),
        scratch_shapes=[pltpu.VMEM((parts, groups * items, 2 * LANES), jnp.bfloat16)],
        compiler_params=PARAMS,
        name="sequence_transform",
    )(
        first_packed,
        in_vmem(values),
        in_vmem(jnp.asarray(np.cos(twiddle), jnp.float32)),
        in_vmem(jnp.asarray(np.sin(twiddle), jnp.float32)),
        in_vmem(jnp.asarray(fine)),
    )


def fold_weights(proj_out, order, group, ranks, chunks):
    count, columns = len(order), proj_out.shape[1]
    table = narrow(unpack_table(group, ranks, chunks))

    def body(order_ref, proj_ref, table_ref, out_ref):
        for at in range(count):
            rows = proj_ref[pl.ds(pl.multiple_of(order_ref[at] * group, group), group), :]
            folded = jnp.dot(table_ref[...], rows, preferred_element_type=jnp.float32)
            out_ref[at * group : (at + 1) * group, :] = folded.astype(jnp.bfloat16)

    return pl.pallas_call(
        body,
        in_specs=[SMEM_SPEC, VMEM_SPEC, VMEM_SPEC],
        out_specs=VMEM_SPEC,
        out_shape=pltpu.VMEM((count * group, columns), jnp.bfloat16),
        compiler_params=PARAMS,
        name="fold_weights",
    )(jnp.stack(order).astype(jnp.int32), in_vmem(proj_out), jnp.asarray(table))


def add_pieces(pieces, weights, first, total, blocks, last):
    count = len(pieces)
    depth = sum(piece.shape[0] for piece in pieces)
    local = pieces[0].shape[1]
    columns = weights.shape[1]
    parts = 8
    groups = local // LANES
    step = next(s for s in (3, 2, 1) if groups % s == 0)
    width = LANES * step

    def body(*refs):
        piece_refs, weight_ref = refs[:count], refs[count]
        out_ref = refs[-1]
        at = pl.ds(pl.multiple_of(pl.program_id(0) * width, width), width)
        lhs = jnp.concatenate([r[:, at] for r in piece_refs], 0)
        rhs = weight_ref[first : first + depth]
        part = lax.dot_general(
            lhs, rhs, (((0,), (0,)), ((), ())), preferred_element_type=jnp.float32
        )
        if total is not None:
            part = part + refs[count + 1][at, :]
        if last:
            for tile in range(step):
                rows = part[tile * LANES : (tile + 1) * LANES].astype(jnp.bfloat16)
                out_ref[:, tile] = rows.reshape(blocks, parts, columns)
        else:
            out_ref[at, :] = part

    if last:
        out_spec = pl.BlockSpec((blocks, step, parts, columns), lambda i: (0, i, 0, 0))
        out_shape = jax.ShapeDtypeStruct((blocks, groups, parts, columns), jnp.bfloat16)
    else:
        out_spec, out_shape = VMEM_SPEC, pltpu.VMEM((local, columns), jnp.float32)
    inputs = [*pieces, weights] + ([] if total is None else [total])
    return pl.pallas_call(
        body,
        grid=(groups // step,),
        in_specs=[VMEM_SPEC] * len(inputs),
        out_specs=out_spec,
        out_shape=out_shape,
        compiler_params=PARAMS,
        name="finish_pieces" if last else "add_pieces",
    )(*map(in_vmem, inputs))


def fast_device(tokens, proj_in, proj_out):
    ranks, _, near = (lax.axis_size(a) for a in (ROW, *COL))
    local = tokens.shape[0]
    group = proj_in.shape[1]
    items = group // ranks
    columns = proj_out.shape[1]
    rank, own = lax.axis_index(ROW), lax.axis_index(COL)
    order = [own, own ^ 1, own ^ near, own ^ near ^ 1]
    blocks = LANES // ranks
    swap = [(i, i ^ 1) for i in range(2)]
    packed = project_in(tokens, proj_in).reshape(ranks, items, local)
    values = lax.all_to_all(packed, ROW, split_axis=0, concat_axis=0, tiled=True)
    first = (rank * items).astype(jnp.int32).reshape(1)
    weights = fold_weights(proj_out, order, group, ranks, CHUNKS)
    found = []
    for c in range(CHUNKS):
        found.append(sequence_transform(values, first, group, c, CHUNKS))
    here, there, here_too, there_too = [], [], [], []
    for c in range(CHUNKS):
        back = lax.all_to_all(found[c], ROW, split_axis=0, concat_axis=0, tiled=True)
        here.append(back.reshape(-1, local))
        there.append(lax.ppermute(here[c], COL[0], swap))
        here_too.append(lax.ppermute(here[c], COL[1], swap))
    total = add_pieces([*here, *here_too], weights, 0, None, blocks, False)
    for c in range(CHUNKS):
        there_too.append(lax.ppermute(there[c], COL[1], swap))
    out = add_pieces([*there, *there_too], weights, 2 * group, total, blocks, True)
    return out.reshape(local, columns)


def solution(mesh):
    ranks, cols = mesh.devices.shape
    near = 2 if cols % 2 == 0 else 1
    inner = Mesh(mesh.devices.reshape(ranks, cols // near, near), (ROW, *COL))

    def program(tokens, proj_in, proj_out):
        local, group = tokens.shape[0] // ranks, proj_in.shape[1] // cols
        fits = (
            group == LANES
            and LANES % ranks == 0
            and ranks % 8 == 0
            and local % LANES == 0
            and near == 2
            and cols == 4
        )
        step = jax.shard_map(
            fast_device if fits else general_device,
            mesh=inner,
            in_specs=(P(ROW, None), P(None, COL), P(None, COL)),
            out_specs=P(ROW, COL),
            check_vma=False,
        )
        return step(tokens, proj_in, proj_out)

    return program
```

profile of v0, /device:TPU:0, one launch (start us, length us, event | category | flops | bytes accessed | tf_op | source)
XLA Modules:
  0.0 49.4 jit_solution(17000426979602362303)
XLA Ops:
  0.0 0.0 copy-start.1
  0.0 0.0 copy-start.2
  0.0 0.0 copy-start.3
  0.0 0.0 copy-start.4
  0.0 6.6 %project_in.1 = bf16[128,1152]{1,0:T(8,128)(2,1)} custom-call(bf16[1152,4096]{1,0:T(8,128)(2,1)} %tokens_ref.1, bf16[4096,128]{1,0:T(8,128)(2,1)} %proj_ref.2, bf16[128,128]{1,0:T(8,128)(2,1)} %constant.30.clone.high_ref, bf16[128,128]{1,0:T(8,128)(2,1)} %constant.31.clone.low_ref), custom_call_target="tpu_custom_call" | custom-call | tf_op jit(solution)/shard_map/project_in/pallas_call | solution.py:256
  6.6 7.3 %all-to-all-start = ((bf16[8,16,1152]{2,1,0:T(8,128)(2,1)}), bf16[8,16,1152]{2,1,0:T(8,128)(2,1)S(1)}, u32[]{:S(2)}, u32[]{:S(2)}) async-start(bf16[8,16,1152]{2,1,0:T(8,128)(2,1)} %bitcast.1), calls=%async_computation | async-start | bytes 589824 | tf_op jit(solution)/shard_map/all_to_all | solution.py:448
  13.9 9.6 %all-to-all-done.values_ref = bf16[8,16,1152]{2,1,0:T(8,128)(2,1)S(1)} async-done(((bf16[8,16,1152]{2,1,0:T(8,128)(2,1)}), bf16[8,16,1152]{2,1,0:T(8,128)(2,1)S(1)}, u32[]{:S(2)}, u32[]{:S(2)}) %all-to-all-start) | async-done | bytes 294944 | tf_op jit(solution)/shard_map/all_to_all | solution.py:448
  23.5 0.0 copy-done.1
  23.5 0.0 copy-done.2
  23.5 0.0 copy-done.3
  23.5 0.9 %sequence_transform.1 = bf16[8,16,1152]{2,1,0:T(8,128)(2,1)S(1)} custom-call(s32[1]{0:T(128)} %bitcast.first_ref, bf16[8,16,1152]{2,1,0:T(8,128)(2,1)S(1)} %all-to-all-done.values_ref, f32[72,128]{1,0:T(8,128)S(1)} %copy-done.3, f32[72,128]{1,0:T(8,128)S(1)} %copy-done.2, bf16[8,256,128]{2,1,0:T(8,128)(2,1)S(1)} %copy-done.1), custom_call_target="tpu_custom_call" | custom-call | tf_op jit(solution)/shard_map/sequence_transform/pallas_call | solution.py:355
  24.4 13.4 %all_to_all.10 = bf16[8,16,1152]{2,1,0:T(8,128)(2,1)S(1)} all-to-all(bf16[8,16,1152]{2,1,0:T(8,128)(2,1)S(1)} %sequence_transform.1), channel_id=1, replica_groups=mesh['row'=8,'far'=2,'near'=2] {'row'}, dimensions={0} | all-to-all | bytes 589824 | tf_op jit(solution)/shard_map/all_to_all | solution.py:456
  37.8 1.5 %collective-permute-start = (bf16[128,1152]{1,0:T(8,128)(2,1)S(1)}, bf16[128,1152]{1,0:T(8,128)(2,1)S(1)}, u32[]{:S(2)}, u32[]{:S(2)}) collective-permute-start(bf16[128,1152]{1,0:T(8,128)(2,1)S(1)} %bitcast.8), channel_id=1, source_target_pairs={{0,2},{2,0},{1,3},{3,1},{4,6},{6,4},{5,7},{7,5},{8,10},{10,8},{9,1... | collective-permute-start | bytes 884744 | tf_op jit(solution)/shard_map/ppermute | solution.py:458
  39.3 0.0 collective-permute-start.2
  39.3 5.2 %collective-permute-done.refs_0_ = bf16[128,1152]{1,0:T(8,128)(2,1)S(1)} collective-permute-done((bf16[128,1152]{1,0:T(8,128)(2,1)S(1)}, bf16[128,1152]{1,0:T(8,128)(2,1)S(1)}, u32[]{:S(2)}, u32[]{:S(2)}) %collective-permute-start) | collective-permute-done | bytes 294944 | tf_op jit(solution)/shard_map/ppermute | solution.py:458
  44.5 0.0 collective-permute-start.1
  44.5 0.1 pad_add_fusion.order_ref
  44.6 0.0 copy-done.4
  44.6 0.0 copy-done
  44.6 1.0 %fold_weights.1.refs_2_ = bf16[512,1024]{1,0:T(8,128)(2,1)S(1)} custom-call(s32[4]{0:T(128)S(1)} %pad_add_fusion.order_ref, bf16[512,1024]{1,0:T(8,128)(2,1)S(1)} %copy-done, bf16[128,128]{1,0:T(8,128)(2,1)S(1)} %copy-done.4), custom_call_target="tpu_custom_call" | custom-call | tf_op jit(solution)/shard_map/fold_weights/pallas_call | solution.py:382
  45.6 0.0 collective-permute-done.2.refs_1_
  45.6 1.2 %add_pieces.1.refs_3_ = f32[1152,1024]{1,0:T(8,128)S(1)} custom-call(bf16[128,1152]{1,0:T(8,128)(2,1)S(1)} %bitcast.10, bf16[128,1152]{1,0:T(8,128)(2,1)S(1)} %collective-permute-done.2.refs_1_, bf16[512,1024]{1,0:T(8,128)(2,1)S(1)} %fold_weights.1.refs_2_), custom_call_target="tpu_custom_call" | custom-call | tf_op jit(solution)/shard_map/add_pieces/pallas_call | solution.py:426
  46.8 0.0 collective-permute-done.1.refs_1_
  46.8 2.6 %finish_pieces.1 = bf16[16,9,8,1024]{3,2,1,0:T(8,128)(2,1)} custom-call(bf16[128,1152]{1,0:T(8,128)(2,1)S(1)} %collective-permute-done.refs_0_, bf16[128,1152]{1,0:T(8,128)(2,1)S(1)} %collective-permute-done.1.refs_1_, bf16[512,1024]{1,0:T(8,128)(2,1)S(1)} %fold_weights.1.refs_2_, f32[1152,1024]{1,0:T(8,128)S(1)} %add_pieces.1.refs_3_), custom_call_target="tpu_custom_call" | custom-call | tf_op jit(solution)/shard_map/finish_pieces/pallas_call | solution.py:426
  (1 shorter events, 0.0 us)
Async XLA Ops:
  0.0 23.5 %copy-start.1 = (bf16[8,256,128]{2,1,0:T(8,128)(2,1)S(1)}, bf16[8,256,128]{2,1,0:T(8,128)(2,1)}, u32[]{:S(2)}) copy-start(bf16[8,256,128]{2,1,0:T(8,128)(2,1)} %constant.35.clone.fine_ref) | copy-start | bytes 1572868
  0.0 23.5 %copy-start.2 = (f32[72,128]{1,0:T(8,128)S(1)}, f32[72,128]{1,0:T(8,128)}, u32[]{:S(2)}) copy-start(f32[72,128]{1,0:T(8,128)} %constant.34.clone.sin_ref) | copy-start | bytes 110596
  0.0 23.5 %copy-start.3 = (f32[72,128]{1,0:T(8,128)S(1)}, f32[72,128]{1,0:T(8,128)}, u32[]{:S(2)}) copy-start(f32[72,128]{1,0:T(8,128)} %constant.33.clone.cos_ref) | copy-start | bytes 110596
  0.0 44.6 %copy-start.4 = (bf16[128,128]{1,0:T(8,128)(2,1)S(1)}, bf16[128,128]{1,0:T(8,128)(2,1)}, u32[]{:S(2)}) copy-start(bf16[128,128]{1,0:T(8,128)(2,1)} %constant.32.clone.table_ref) | copy-start | bytes 98308
  0.0 44.6 %copy-start = (bf16[512,1024]{1,0:T(8,128)(2,1)S(1)}, bf16[512,1024]{1,0:T(8,128)(2,1)}, u32[]{:S(2)}) copy-start(bf16[512,1024]{1,0:T(8,128)(2,1)} %proj_ref.3) | copy-start | bytes 3145732
  6.6 16.9 %all-to-all-start = ((bf16[8,16,1152]{2,1,0:T(8,128)(2,1)}), bf16[8,16,1152]{2,1,0:T(8,128)(2,1)S(1)}, u32[]{:S(2)}, u32[]{:S(2)}) async-start(bf16[8,16,1152]{2,1,0:T(8,128)(2,1)} %bitcast.1), calls=%async_computation | async-start | bytes 589824 | tf_op jit(solution)/shard_map/all_to_all | solution.py:448
  37.8 6.7 %collective-permute-start = (bf16[128,1152]{1,0:T(8,128)(2,1)S(1)}, bf16[128,1152]{1,0:T(8,128)(2,1)S(1)}, u32[]{:S(2)}, u32[]{:S(2)}) collective-permute-start(bf16[128,1152]{1,0:T(8,128)(2,1)S(1)} %bitcast.8), channel_id=1, source_target_pairs={{0,2},{2,0},{1,3},{3,1},{4,6},{6,4},{5,7},{7,5},{8,10},{10,8},{9,1... | collective-permute-start | bytes 884744 | tf_op jit(solution)/shard_map/ppermute | solution.py:458
  39.3 6.3 %collective-permute-start.2 = (bf16[128,1152]{1,0:T(8,128)(2,1)S(1)}, bf16[128,1152]{1,0:T(8,128)(2,1)S(1)}, u32[]{:S(2)}, u32[]{:S(2)}) collective-permute-start(bf16[128,1152]{1,0:T(8,128)(2,1)S(1)} %bitcast.9), channel_id=1, source_target_pairs={{0,1},{1,0},{2,3},{3,2},{4,5},{5,4},{6,7},{7,6},{8,9},{9,8},{10,11... | collective-permute-start | bytes 884744 | tf_op jit(solution)/shard_map/ppermute | solution.py:459
  44.5 2.3 %collective-permute-start.1 = (bf16[128,1152]{1,0:T(8,128)(2,1)S(1)}, bf16[128,1152]{1,0:T(8,128)(2,1)S(1)}, u32[]{:S(2)}, u32[]{:S(2)}) collective-permute-start(bf16[128,1152]{1,0:T(8,128)(2,1)S(1)} %collective-permute-done.refs_0_), channel_id=1, source_target_pairs={{0,1},{1,0},{2,3},{3,2},{4,5},{5,4},{6,7},{7,6},{8,9},{9,8},{10,11... | collective-permute-start | bytes 884744 | tf_op jit(solution)/shard_map/ppermute | solution.py:462
where the time goes:
time: 49.7 us; the launch traced here: 49.4 us
  waiting for transfers between devices  14.8 us (30%)
  blocking collectives  13.4 us (27%)
  Pallas kernels  12.3 us (25%)
  starting transfers between devices  8.81 us (18%)
    all_to_all x1, blocking collectives, fast_device(): lax.all_to_all(found[c], ROW, split_axis=0, concat_axis=0, tiled=True)  13.4 us
    all_to_all x1, waiting for transfers between devices, fast_device(): lax.all_to_all(packed, ROW, split_axis=0, concat_axis=0, tiled=True)  9.61 us
    all_to_all x1, starting transfers between devices, fast_device(): lax.all_to_all(packed, ROW, split_axis=0, concat_axis=0, tiled=True)  7.29 us
    pallas_call x1, Pallas kernels, project_in(): pl.pallas_call(body, grid=(steps,), in_specs=[pl.BlockSpec((rows, depth),...  6.61 us
    ppermute x1, waiting for transfers between devices, fast_device(): there.append(lax.ppermute(here[c], COL[0], swap))  5.2 us
    pallas_call x2, Pallas kernels, add_pieces(): pl.pallas_call(body, grid=(groups // step,), in_specs=[VMEM_SPEC] * len(i...  3.8 us
    ppermute x1, starting transfers between devices, fast_device(): there.append(lax.ppermute(here[c], COL[0], swap))  1.52 us
  transfers between devices with their start and end apart: 4, of which 2 were waited for; matrix products, arithmetic and copies ran while one was open for 0% of the time, Pallas kernels for 4%

commit v1 on v0

--- a/solution.py
+++ b/solution.py
@@ -262,8 +262,8 @@
             pl.BlockSpec((group, group), whole),
             pl.BlockSpec((group, group), whole),
         ],
-        out_specs=pl.BlockSpec((group, rows), whole),
-        out_shape=jax.ShapeDtypeStruct((group, rows), jnp.bfloat16),
+        out_specs=VMEM_SPEC,
+        out_shape=pltpu.VMEM((group, rows), jnp.bfloat16),
         scratch_shapes=[pltpu.VMEM((rows, group), jnp.float32)],
         compiler_params=PARAMS,
         name="project_in",
@@ -396,39 +396,49 @@
     columns = weights.shape[1]
     parts = 8
     groups = local // LANES
-    step = next(s for s in (3, 2, 1) if groups % s == 0)
-    width = LANES * step
-
-    def body(*refs):
-        piece_refs, weight_ref = refs[:count], refs[count]
-        out_ref = refs[-1]
-        at = pl.ds(pl.multiple_of(pl.program_id(0) * width, width), width)
-        lhs = jnp.concatenate([r[:, at] for r in piece_refs], 0)
-        rhs = weight_ref[first : first + depth]
-        part = lax.dot_general(
+
+    def product(refs, at):
+        lhs = jnp.concatenate([r[:, at] for r in refs[:count]], 0)
+        rhs = refs[count][first : first + depth]
+        return lax.dot_general(
             lhs, rhs, (((0,), (0,)), ((), ())), preferred_element_type=jnp.float32
         )
-        if total is not None:
-            part = part + refs[count + 1][at, :]
-        if last:
-            for tile in range(step):
-                rows = part[tile * LANES : (tile + 1) * LANES].astype(jnp.bfloat16)
-                out_ref[:, tile] = rows.reshape(blocks, parts, columns)
-        else:
-            out_ref[at, :] = part
-
-    if last:
-        out_spec = pl.BlockSpec((blocks, step, parts, columns), lambda i: (0, i, 0, 0))
-        out_shape = jax.ShapeDtypeStruct((blocks, groups, parts, columns), jnp.bfloat16)
-    else:
-        out_spec, out_shape = VMEM_SPEC, pltpu.VMEM((local, columns), jnp.float32)
+
+    def start(*refs):
+        for tile in range(groups):
+            at = pl.ds(tile * LANES, LANES)
+            refs[-1][at, :] = product(refs, at)
+
+    def finish(*refs):
+        total_ref, out_ref, rows_ref, sem_ref = refs[-4:]
+        copies = []
+        for tile in range(groups):
+            at = pl.ds(tile * LANES, LANES)
+            rows = (product(refs, at) + total_ref[at, :]).astype(jnp.bfloat16)
+            rows_ref[tile] = rows.reshape(blocks, parts, columns)
+            copies.append(
+                pltpu.make_async_copy(rows_ref.at[tile], out_ref.at[:, tile], sem_ref.at[tile])
+            )
+            copies[-1].start()
+        for copy in copies:
+            copy.wait()
+
     inputs = [*pieces, weights] + ([] if total is None else [total])
+    shape = (blocks, groups, parts, columns)
+    scratch = [
+        pltpu.VMEM((groups, blocks, parts, columns), jnp.bfloat16),
+        pltpu.SemaphoreType.DMA((groups,)),
+    ]
     return pl.pallas_call(
-        body,
-        grid=(groups // step,),
+        finish if last else start,
         in_specs=[VMEM_SPEC] * len(inputs),
-        out_specs=out_spec,
-        out_shape=out_shape,
+        out_specs=pl.BlockSpec(memory_space=pl.ANY) if last else VMEM_SPEC,
+        out_shape=(
+            jax.ShapeDtypeStruct(shape, jnp.bfloat16)
+            if last
+            else pltpu.VMEM((local, columns), jnp.float32)
+        ),
+        scratch_shapes=scratch if last else [],
         compiler_params=PARAMS,
         name="finish_pieces" if last else "add_pieces",
     )(*map(in_vmem, inputs))

time: 49.7 us -> 48.4 us (0.974)
  Pallas kernels: 12.3 us -> 11 us
    pallas_call x2, Pallas kernels: 3.8 us -> 2.55 us  [add_pieces(): pl.pallas_call(finish if last else start, in_specs=[VMEM_SPEC] * len(inpu...]
where the time goes in v1:
time: 48.4 us; the launch traced here: 48.2 us
  waiting for transfers between devices  14.8 us (31%)
  blocking collectives  13.4 us (28%)
  Pallas kernels  11 us (23%)
  starting transfers between devices  8.81 us (18%)
    all_to_all x1, blocking collectives, fast_device(): lax.all_to_all(found[c], ROW, split_axis=0, concat_axis=0, tiled=True)  13.4 us
    all_to_all x1, waiting for transfers between devices, fast_device(): lax.all_to_all(packed, ROW, split_axis=0, concat_axis=0, tiled=True)  9.61 us
    all_to_all x1, starting transfers between devices, fast_device(): lax.all_to_all(packed, ROW, split_axis=0, concat_axis=0, tiled=True)  7.29 us
    pallas_call x1, Pallas kernels, project_in(): pl.pallas_call(body, grid=(steps,), in_specs=[pl.BlockSpec((rows, depth),...  6.61 us
    ppermute x1, waiting for transfers between devices, fast_device(): there.append(lax.ppermute(here[c], COL[0], swap))  5.2 us
    pallas_call x2, Pallas kernels, add_pieces(): pl.pallas_call(finish if last else start, in_specs=[VMEM_SPEC] * len(inpu...  2.55 us
    ppermute x1, starting transfers between devices, fast_device(): there.append(lax.ppermute(here[c], COL[0], swap))  1.52 us
  transfers between devices with their start and end apart: 4, of which 2 were waited for; matrix products, arithmetic and copies ran while one was open for 0% of the time, Pallas kernels for 4%

profile of v1, /device:TPU:0, one launch (start us, length us, event | category | flops | bytes accessed | tf_op | source)
XLA Modules:
  0.0 48.2 jit_solution(12711891314536331021)
XLA Ops:
  0.0 0.0 copy-start.1
  0.0 0.0 copy-start.2
  0.0 0.0 copy-start.3
  0.0 0.0 copy-start.4
  0.0 6.6 %project_in.1 = bf16[128,1152]{1,0:T(8,128)(2,1)} custom-call(bf16[1152,4096]{1,0:T(8,128)(2,1)} %tokens_ref.1, bf16[4096,128]{1,0:T(8,128)(2,1)} %proj_ref.2, bf16[128,128]{1,0:T(8,128)(2,1)} %constant.30.clone.high_ref, bf16[128,128]{1,0:T(8,128)(2,1)} %constant.31.clone.low_ref), custom_call_target="tpu_custom_call" | custom-call | tf_op jit(solution)/shard_map/project_in/pallas_call | solution.py:256
  6.6 7.3 %all-to-all-start = ((bf16[8,16,1152]{2,1,0:T(8,128)(2,1)}), bf16[8,16,1152]{2,1,0:T(8,128)(2,1)S(1)}, u32[]{:S(2)}, u32[]{:S(2)}) async-start(bf16[8,16,1152]{2,1,0:T(8,128)(2,1)} %bitcast.1), calls=%async_computation | async-start | bytes 589824 | tf_op jit(solution)/shard_map/all_to_all | solution.py:458
  13.9 9.6 %all-to-all-done.values_ref = bf16[8,16,1152]{2,1,0:T(8,128)(2,1)S(1)} async-done(((bf16[8,16,1152]{2,1,0:T(8,128)(2,1)}), bf16[8,16,1152]{2,1,0:T(8,128)(2,1)S(1)}, u32[]{:S(2)}, u32[]{:S(2)}) %all-to-all-start) | async-done | bytes 294944 | tf_op jit(solution)/shard_map/all_to_all | solution.py:458
  23.5 0.0 copy-done.1
  23.5 0.0 copy-done.2
  23.5 0.0 copy-done.3
  23.5 0.9 %sequence_transform.1 = bf16[8,16,1152]{2,1,0:T(8,128)(2,1)S(1)} custom-call(s32[1]{0:T(128)} %bitcast.first_ref, bf16[8,16,1152]{2,1,0:T(8,128)(2,1)S(1)} %all-to-all-done.values_ref, f32[72,128]{1,0:T(8,128)S(1)} %copy-done.3, f32[72,128]{1,0:T(8,128)S(1)} %copy-done.2, bf16[8,256,128]{2,1,0:T(8,128)(2,1)S(1)} %copy-done.1), custom_call_target="tpu_custom_call" | custom-call | tf_op jit(solution)/shard_map/sequence_transform/pallas_call | solution.py:355
  24.4 13.4 %all_to_all.10 = bf16[8,16,1152]{2,1,0:T(8,128)(2,1)S(1)} all-to-all(bf16[8,16,1152]{2,1,0:T(8,128)(2,1)S(1)} %sequence_transform.1), channel_id=1, replica_groups=mesh['row'=8,'far'=2,'near'=2] {'row'}, dimensions={0} | all-to-all | bytes 589824 | tf_op jit(solution)/shard_map/all_to_all | solution.py:466
  37.8 1.5 %collective-permute-start = (bf16[128,1152]{1,0:T(8,128)(2,1)S(1)}, bf16[128,1152]{1,0:T(8,128)(2,1)S(1)}, u32[]{:S(2)}, u32[]{:S(2)}) collective-permute-start(bf16[128,1152]{1,0:T(8,128)(2,1)S(1)} %bitcast.8), channel_id=1, source_target_pairs={{0,2},{2,0},{1,3},{3,1},{4,6},{6,4},{5,7},{7,5},{8,10},{10,8},{9,1... | collective-permute-start | bytes 884744 | tf_op jit(solution)/shard_map/ppermute | solution.py:468
  39.3 0.0 collective-permute-start.2
  39.3 5.2 %collective-permute-done.refs_0_ = bf16[128,1152]{1,0:T(8,128)(2,1)S(1)} collective-permute-done((bf16[128,1152]{1,0:T(8,128)(2,1)S(1)}, bf16[128,1152]{1,0:T(8,128)(2,1)S(1)}, u32[]{:S(2)}, u32[]{:S(2)}) %collective-permute-start) | collective-permute-done | bytes 294944 | tf_op jit(solution)/shard_map/ppermute | solution.py:468
  44.5 0.0 collective-permute-start.1
  44.5 0.1 pad_add_fusion.order_ref
  44.6 0.0 copy-done.4
  44.6 0.0 copy-done
  44.6 1.0 %fold_weights.1.refs_2_ = bf16[512,1024]{1,0:T(8,128)(2,1)S(1)} custom-call(s32[4]{0:T(128)S(1)} %pad_add_fusion.order_ref, bf16[512,1024]{1,0:T(8,128)(2,1)S(1)} %copy-done, bf16[128,128]{1,0:T(8,128)(2,1)S(1)} %copy-done.4), custom_call_target="tpu_custom_call" | custom-call | tf_op jit(solution)/shard_map/fold_weights/pallas_call | solution.py:382
  45.6 0.0 collective-permute-done.2.refs_1_
  45.6 0.8 %add_pieces.1.refs_3_ = f32[1152,1024]{1,0:T(8,128)S(1)} custom-call(bf16[128,1152]{1,0:T(8,128)(2,1)S(1)} %bitcast.10, bf16[128,1152]{1,0:T(8,128)(2,1)S(1)} %collective-permute-done.2.refs_1_, bf16[512,1024]{1,0:T(8,128)(2,1)S(1)} %fold_weights.1.refs_2_), custom_call_target="tpu_custom_call" | custom-call | tf_op jit(solution)/shard_map/add_pieces/pallas_call | solution.py:432
  46.4 0.0 collective-permute-done.1.refs_1_
  46.4 1.7 %finish_pieces.1 = bf16[16,9,8,1024]{3,2,1,0:T(8,128)(2,1)} custom-call(bf16[128,1152]{1,0:T(8,128)(2,1)S(1)} %collective-permute-done.refs_0_, bf16[128,1152]{1,0:T(8,128)(2,1)S(1)} %collective-permute-done.1.refs_1_, bf16[512,1024]{1,0:T(8,128)(2,1)S(1)} %fold_weights.1.refs_2_, f32[1152,1024]{1,0:T(8,128)S(1)} %add_pieces.1.refs_3_), custom_call_target="tpu_custom_call" | custom-call | tf_op jit(solution)/shard_map/finish_pieces/pallas_call | solution.py:432
  (1 shorter events, 0.0 us)
Async XLA Ops:
  0.0 23.5 %copy-start.1 = (bf16[8,256,128]{2,1,0:T(8,128)(2,1)S(1)}, bf16[8,256,128]{2,1,0:T(8,128)(2,1)}, u32[]{:S(2)}) copy-start(bf16[8,256,128]{2,1,0:T(8,128)(2,1)} %constant.35.clone.fine_ref) | copy-start | bytes 1572868
  0.0 23.5 %copy-start.2 = (f32[72,128]{1,0:T(8,128)S(1)}, f32[72,128]{1,0:T(8,128)}, u32[]{:S(2)}) copy-start(f32[72,128]{1,0:T(8,128)} %constant.34.clone.sin_ref) | copy-start | bytes 110596
  0.0 23.5 %copy-start.3 = (f32[72,128]{1,0:T(8,128)S(1)}, f32[72,128]{1,0:T(8,128)}, u32[]{:S(2)}) copy-start(f32[72,128]{1,0:T(8,128)} %constant.33.clone.cos_ref) | copy-start | bytes 110596
  0.0 44.6 %copy-start.4 = (bf16[128,128]{1,0:T(8,128)(2,1)S(1)}, bf16[128,128]{1,0:T(8,128)(2,1)}, u32[]{:S(2)}) copy-start(bf16[128,128]{1,0:T(8,128)(2,1)} %constant.32.clone.table_ref) | copy-start | bytes 98308
  0.0 44.6 %copy-start = (bf16[512,1024]{1,0:T(8,128)(2,1)S(1)}, bf16[512,1024]{1,0:T(8,128)(2,1)}, u32[]{:S(2)}) copy-start(bf16[512,1024]{1,0:T(8,128)(2,1)} %proj_ref.3) | copy-start | bytes 3145732
  6.6 16.9 %all-to-all-start = ((bf16[8,16,1152]{2,1,0:T(8,128)(2,1)}), bf16[8,16,1152]{2,1,0:T(8,128)(2,1)S(1)}, u32[]{:S(2)}, u32[]{:S(2)}) async-start(bf16[8,16,1152]{2,1,0:T(8,128)(2,1)} %bitcast.1), calls=%async_computation | async-start | bytes 589824 | tf_op jit(solution)/shard_map/all_to_all | solution.py:458
  37.8 6.7 %collective-permute-start = (bf16[128,1152]{1,0:T(8,128)(2,1)S(1)}, bf16[128,1152]{1,0:T(8,128)(2,1)S(1)}, u32[]{:S(2)}, u32[]{:S(2)}) collective-permute-start(bf16[128,1152]{1,0:T(8,128)(2,1)S(1)} %bitcast.8), channel_id=1, source_target_pairs={{0,2},{2,0},{1,3},{3,1},{4,6},{6,4},{5,7},{7,5},{8,10},{10,8},{9,1... | collective-permute-start | bytes 884744 | tf_op jit(solution)/shard_map/ppermute | solution.py:468
  39.3 6.3 %collective-permute-start.2 = (bf16[128,1152]{1,0:T(8,128)(2,1)S(1)}, bf16[128,1152]{1,0:T(8,128)(2,1)S(1)}, u32[]{:S(2)}, u32[]{:S(2)}) collective-permute-start(bf16[128,1152]{1,0:T(8,128)(2,1)S(1)} %bitcast.9), channel_id=1, source_target_pairs={{0,1},{1,0},{2,3},{3,2},{4,5},{5,4},{6,7},{7,6},{8,9},{9,8},{10,11... | collective-permute-start | bytes 884744 | tf_op jit(solution)/shard_map/ppermute | solution.py:469
  44.5 1.9 %collective-permute-start.1 = (bf16[128,1152]{1,0:T(8,128)(2,1)S(1)}, bf16[128,1152]{1,0:T(8,128)(2,1)S(1)}, u32[]{:S(2)}, u32[]{:S(2)}) collective-permute-start(bf16[128,1152]{1,0:T(8,128)(2,1)S(1)} %collective-permute-done.refs_0_), channel_id=1, source_target_pairs={{0,1},{1,0},{2,3},{3,2},{4,5},{5,4},{6,7},{7,6},{8,9},{9,8},{10,11... | collective-permute-start | bytes 884744 | tf_op jit(solution)/shard_map/ppermute | solution.py:472
